TPU v7x, 32 devices: a whole 2x2x4 slice. The times are simulated.
32 devices in a mesh: sp: 8 (over z, y), tp: 4 (over x, core).
Axes of the slice: x: 2, y: 2, z: 4, core: 2. Of those that a mesh axis runs over, the one named last changes fastest.
Arguments:
- tokens: bfloat16 [2048, 1024], P(('sp', 'tp')), may hold values from -7.5 to 7.5, as said below
- query_weight: bfloat16 [1024, 2048], P('sp', 'tp'), may hold values from -0.1875 to 0.1875
- key_weight: bfloat16 [1024, 2048], P('sp', 'tp'), may hold values from -0.1875 to 0.1875
- value_weight: bfloat16 [1024, 2048], P('sp', 'tp'), may hold values from -0.1875 to 0.1875
- gate_weight: bfloat16 [1024, 16], P('sp', 'tp'), may hold values from -0.1875 to 0.1875
- forget_bias: float32 [16], P('tp'), may hold values from 0 to 2
- out_weight: bfloat16 [2048, 1024], P('tp', 'sp'), may hold values from -0.125 to 0.125
- out_gain: float32 [1024], replicated, may hold values from 0.5 to 1.5
Outputs:
- mixed: bfloat16 [2048, 1024], P(('sp', 'tp'))
Inputs may be any that keep to these rules, and one draw needn't show every extreme that they name: `tokens`: each entry is a bounded noise value (at most 6 in size) plus an offset in -1.5 to 1.5 shared by the 256 rows of one index of sp, so every entry lies within -7.5 and 7.5.
All inputs are finite; a program needn't handle non-finite values.
Results may differ from a plain program's by a relative error of at most 0.006.
Values may be sent and summed in bfloat16 or wider, within the bound.
A program may use at most 128 MiB of HBM per device.

v0:
```python
import math
import jax
import jax.numpy as jnp
from jax import lax
from jax.sharding import PartitionSpec as P


def on_whole(shard, axis, dim, block):
    whole = lax.all_gather(shard, axis, axis=dim, tiled=True)
    return block(whole, jnp.int32(0))


def over_all(shard, axis, dim, absorb, state):
    everything = jax.tree.map(lambda a: lax.all_gather(a, axis, axis=dim, tiled=True), shard)
    return absorb(state, everything, jnp.int32(0))


def own_rows(product, width, axis):
    everything = product(jnp.int32(0), lax.axis_size(axis) * width)
    own = lax.psum_scatter(everything, axis, scatter_dimension=0, tiled=True)
    return own


def on_device(
    tokens, query_weight, key_weight, value_weight, gate_weight, forget_bias, out_weight, out_gain
):
    width = query_weight.shape[1]
    heads = gate_weight.shape[1]
    head_size = width // heads
    whole_q = lax.all_gather(query_weight, "sp", axis=0, tiled=True)
    whole_k = lax.all_gather(key_weight, "sp", axis=0, tiled=True)
    whole_v = lax.all_gather(value_weight, "sp", axis=0, tiled=True)
    whole_g = lax.all_gather(gate_weight, "sp", axis=0, tiled=True)
    joined = jnp.concatenate([whole_q, whole_k, whole_v, whole_g], axis=1)

    def project(piece, start):
        return jnp.dot(piece, joined, preferred_element_type=jnp.float32)

    projected = on_whole(tokens, "tp", 0, project)
    block = projected.shape[0]
    queries = projected[:, :width].astype(jnp.bfloat16).reshape(block, heads, head_size)
    keys = projected[:, width : 2 * width].astype(jnp.bfloat16).reshape(block, heads, head_size)
    values = (
        projected[:, 2 * width : 3 * width].astype(jnp.bfloat16).reshape(block, heads, head_size)
    )
    seq_len = block * lax.axis_size("sp")
    log_gate = jax.nn.log_sigmoid(projected[:, 3 * width :] + forget_bias + math.log(seq_len))
    gates_all = lax.all_gather(log_gate, "sp", axis=0, tiled=True)
    cumulative = jnp.cumsum(gates_all, axis=0)
    first = lax.axis_index("sp") * block
    query_cum = lax.dynamic_slice_in_dim(cumulative, first, block, 0)
    query_pos = first + jnp.arange(block, dtype=jnp.int32)
    scale = head_size ** (-0.5)

    def update(carry, piece, start):
        run_max, run_sum, run_acc = carry
        key_piece, value_piece = piece
        length = key_piece.shape[0]
        key_cum = lax.dynamic_slice_in_dim(cumulative, start, length, 0)
        logits = (
            jnp.einsum("qhd,khd->hqk", queries, key_piece, preferred_element_type=jnp.float32)
            * scale
        )
        logits = logits + query_cum.T[:, :, None] - key_cum.T[:, None, :]
        key_pos = start + jnp.arange(length, dtype=jnp.int32)
        allowed = (key_pos[None, :] <= query_pos[:, None])[None]
        logits = jnp.where(allowed, logits, -1e30)
        new_max = jnp.maximum(run_max, jnp.max(logits, axis=-1))
        probs = jnp.where(allowed, jnp.exp(logits - new_max[..., None]), 0.0)
        factor = jnp.exp(run_max - new_max)
        new_sum = run_sum * factor + jnp.sum(probs, axis=-1)
        new_acc = run_acc * factor[..., None] + jnp.einsum(
            "hqk,khd->hqd", probs, value_piece.astype(jnp.float32)
        )
        return (new_max, new_sum, new_acc)

    def attend(carry, piece, start):
        return lax.cond(
            start > first + block - 1,
            lambda state: state,
            lambda state: update(state, piece, start),
            carry,
        )

    initial = (
        jnp.full((heads, block), -1e30, jnp.float32),
        jnp.zeros((heads, block), jnp.float32),
        jnp.zeros((heads, block, head_size), jnp.float32),
    )
    run_max, run_sum, run_acc = over_all((keys, values), "sp", 0, attend, initial)
    attended = (
        (run_acc / run_sum[..., None]).transpose(1, 0, 2).reshape(block, width).astype(jnp.bfloat16)
    )
    out_full = lax.all_gather(out_weight, "sp", axis=1, tiled=True)
    rows = tokens.shape[0]

    def term(start, count):
        return jnp.dot(
            lax.dynamic_slice_in_dim(attended, start, count, 0),
            out_full,
            preferred_element_type=jnp.float32,
        )

    summed = own_rows(term, rows, "tp")
    normed = summed * lax.rsqrt(jnp.mean(summed * summed, axis=-1, keepdims=True) + 1e-06)
    return (normed * out_gain).astype(jnp.bfloat16)


def solution(mesh):
    placed = (
        P(("sp", "tp"), None),
        P("sp", "tp"),
        P("sp", "tp"),
        P("sp", "tp"),
        P("sp", "tp"),
        P("tp"),
        P("tp", "sp"),
        P(),
    )
    return jax.shard_map(
        on_device, mesh=mesh, in_specs=placed, out_specs=P(("sp", "tp"), None), check_vma=False
    )
```

profile of v0, /device:TPU:0, one launch (start us, length us, event | category | flops | bytes accessed | tf_op | source)
XLA Modules:
  0.0 312.7 jit_solution(10969626571004091959)
XLA Ops:
  6.5 0.0 all-gather.11.cloned.1.call-start
  6.5 0.7 all-gather.11.cloned.1.call-update
  7.3 0.0 all-gather.9.cloned.1.call-start
  7.3 0.7 all-gather.9.cloned.1.call-update
  8.0 0.0 all-gather.7.cloned.1.call-start
  8.1 0.7 all-gather.7.cloned.1.call-update
  8.7 0.0 all-gather.13.cloned.1.call-start
  8.8 22.6 %all_gather.30 = bf16[1024,4]{0,1:T(4,128)(2,1)S(1)} all-gather(bf16[128,4]{0,1:T(4,128)(2,1)} %param.14), channel_id=1, replica_groups=mesh['sp'=8,'tp'=4] {'sp'}, dimensions={0}, use_global_device_ids=true | all-gather | bytes 9216 | tf_op jit(solution)/shard_map/all_gather | solution.py:33
  31.4 0.2 copy.14
  31.6 7.4 %all_gather.31 = bf16[256,1024]{1,0:T(8,128)(2,1)S(1)} all-gather(bf16[64,1024]{1,0:T(8,128)(2,1)} %param.10), channel_id=1, replica_groups=mesh['sp'=8,'tp'=4] {'tp'}, dimensions={0}, use_global_device_ids=true | all-gather | bytes 655360 | tf_op jit(solution)/shard_map/all_gather | solution.py:9
  38.9 0.0 copy-start.1
  39.0 13.5 %all-gather.11.cloned.1.call-done = bf16[1024,512]{1,0:T(8,128)(2,1)} async-done(((bf16[128,512]{1,0:T(8,128)(2,1)}), bf16[1024,512]{1,0:T(8,128)(2,1)}) %all-gather.11.cloned.1.call-update) | async-done | bytes 1048592 | tf_op jit(solution)/shard_map/all_gather | solution.py:32
  52.5 41.1 %all-gather.9.cloned.1.call-done = bf16[1024,512]{1,0:T(8,128)(2,1)} async-done(((bf16[128,512]{1,0:T(8,128)(2,1)}), bf16[1024,512]{1,0:T(8,128)(2,1)}) %all-gather.9.cloned.1.call-update) | async-done | bytes 1048592 | tf_op jit(solution)/shard_map/all_gather | solution.py:31
  93.6 41.2 %all-gather.7.cloned.1.call-done = bf16[1024,512]{1,0:T(8,128)(2,1)} async-done(((bf16[128,512]{1,0:T(8,128)(2,1)}), bf16[1024,512]{1,0:T(8,128)(2,1)}) %all-gather.7.cloned.1.call-update) | async-done | bytes 1048592 | tf_op jit(solution)/shard_map/all_gather | solution.py:30
  134.8 2.9 fusion.32
  137.8 0.9 copy.15
  138.6 0.0 all-gather.13.cloned.1.call-update
  138.7 0.0 all-gather.15.cloned.1.call-start
  138.7 0.8 copy.16
  139.6 0.0 all-gather.15.cloned.1.call-update
  139.6 0.0 all-gather.17.cloned.1.call-start
  139.6 0.5 all-gather.17.cloned.1.call-update
  140.2 0.0 reduce-scatter.2.cloned.1.call-start
  140.2 0.0 copy-done.1
  140.2 0.1 fusion.26
  140.3 31.0 %all_gather.33 = f32[2048,4]{0,1:T(4,128)S(1)} all-gather(f32[256,4]{0,1:T(4,128)S(1)} %fusion.26), channel_id=1, replica_groups=mesh['sp'=8,'tp'=4] {'sp'}, dimensions={0}, use_global_device_ids=true | all-gather | bytes 36864 | tf_op jit(solution)/shard_map/all_gather | solution.py:48
  171.3 1.1 reduce-window.6
  172.4 0.2 slice_reduce_fusion
  172.6 0.2 reduce-window.9
  172.8 0.1 add_bitcast_fusion
  172.9 13.9 %all-gather.13.cloned.1.call-done = bf16[2048,4,128]{2,0,1:T(8,128)(2,1)} async-done(((bf16[256,4,128]{2,0,1:T(8,128)(2,1)}), bf16[2048,4,128]{2,0,1:T(8,128)(2,1)}) %all-gather.13.cloned.1.call-update) | async-done | bytes 2097168 | tf_op jit(solution)/shard_map/all_gather | solution.py:14
  186.9 49.7 %all-gather.15.cloned.1.call-done = bf16[2048,4,128]{2,0,1:T(8,128)(2,1)} async-done(((bf16[256,4,128]{2,0,1:T(8,128)(2,1)}), bf16[2048,4,128]{2,0,1:T(8,128)(2,1)}) %all-gather.15.cloned.1.call-update) | async-done | bytes 2097168 | tf_op jit(solution)/shard_map/all_gather | solution.py:14
  236.6 0.0 copy-start
  236.6 11.8 %conditional.1 = (f32[4,256]{1,0:T(4,128)S(1)}, f32[4,256,128]{1,2,0:T(8,128)S(1)}) conditional(s32[]{:T(128)} %convert_element_type.19, (s32[]{:T(128)}, s32[256]{0:T(256)S(1)}, bf16[256,1540]{0,1:T(8,128)(2,1)S(1)}, bf16[2048,4,128]{2,0,1:T(8,128)(2,1)}, f32[256,4]{0,1:T(4,128)S(1)}, /*index=5*/f32[2048,4]{0,1:T(4,128)S(1)}, ...), branch_computations={%region_2.5_spmd, %region_5.6_spmd} | conditional | flops 1112149248 | bytes 42363952 | solution.py:78
  236.6 0.4 iota_compare_fusion
  237.0 0.0 copy-start.2
  237.0 4.6 %fusion.2 = (f32[4,256]{1,0:T(4,128)S(1)}, f32[4,256,2048]{2,1,0:T(8,128)S(1)}) fusion(f32[4,2048]{1,0:T(4,128)S(1)} %bitcast.40, f32[4,256]{1,0:T(4,128)S(1)} %bitcast.45, pred[256,2048]{1,0:T(8,128)(4,1)S(1)} %iota_compare_fusion, bf16[256,4,128]{0,2,1:T(8,128)(2,1)S(1)} %bitcast.37, bf16[2048,4,128]{2,0,1:T(8,128)(2,1)} %get-tuple-element.25), kind=kOutput, calls=%fused_computation.4 | convolution fusion | flops 547355648 | bytes 11313152 | tf_op jit(solution)/shard_map/cond/branch_0_fun/qhd,khd->hqk/dot_general | solution.py:61
  241.7 3.2 %fusion.1 = f32[4,256]{1,0:T(4,128)S(1)} fusion(f32[4,256,2048]{2,1,0:T(8,128)S(1)} %get-tuple-element.45, f32[4,256]{1,0:T(4,128)S(1)} %broadcast_maximum_fusion, f32[4,2048]{1,0:T(4,128)S(1)} %bitcast.41, f32[4,256]{1,0:T(4,128)S(1)} %bitcast.46, pred[256,2048]{1,0:T(8,128)(4,1)S(1)} %iota_compare_fusion), kind=kLoop, calls=%fused_computation.3 | loop fusion | flops 14679040 | bytes 8957952 | tf_op jit(solution)/shard_map/cond/branch_0_fun/reduce_sum | solution.py:71
  244.9 0.0 copy-done.2
  244.9 3.3 %fusion.10 = f32[4,256,128]{2,1,0:T(8,128)S(1)} fusion(bf16[2048,4,128]{2,0,1:T(8,128)(2,1)S(1)} %copy-done.2, f32[4,256,2048]{2,1,0:T(8,128)S(1)} %get-tuple-element.45, f32[4,256]{1,0:T(4,128)S(1)} %broadcast_maximum_fusion, f32[4,2048]{1,0:T(4,128)S(1)} %bitcast.42, f32[4,256]{1,0:T(4,128)S(1)} %bitcast.47, pred[256,2048]{1,0:T(8,128)(4,1)S(1)} %iota_compare_fusion, ...), kind=kOutput, calls=%fused_computation.13 | convolution fusion | flops 549584896 | bytes 11579392 | tf_op jit(solution)/shard_map/cond/branch_0_fun/hqk,khd->hqd/dot_general | solution.py:72
  248.1 0.2 copy.19
  248.4 28.0 %all-gather.17.cloned.1.call-done = bf16[512,1024]{1,0:T(8,128)(2,1)} async-done(((bf16[512,128]{1,0:T(8,128)(2,1)}), bf16[512,1024]{1,0:T(8,128)(2,1)}) %all-gather.17.cloned.1.call-update) | async-done | bytes 1048592 | tf_op jit(solution)/shard_map/all_gather | solution.py:94
  276.5 2.7 fusion.33
  279.1 0.0 reduce-scatter.2.cloned.1.call-update
  279.1 24.0 %reduce-scatter.2.cloned.1.call-done = f32[64,1024]{1,0:T(8,128)} async-done(((f32[256,1024]{1,0:T(8,128)}), f32[64,1024]{1,0:T(8,128)}) %reduce-scatter.2.cloned.1.call-update) | async-done | bytes 262160 | tf_op jit(solution)/shard_map/reduce_scatter | solution.py:20
  303.1 1.1 multiply_reduce_fusion
  304.2 0.0 copy-done
  304.2 1.7 multiply_convert_fusion
  (11 shorter events, 0.2 us)
Async XLA Ops:
  6.5 46.0 %all-gather.11.cloned.1.call-start = ((), (), s32[]{:S(2)}) async-start(), calls=%async_computation.3 | async-start | bytes 1179648 | tf_op jit(solution)/shard_map/all_gather | solution.py:32
  7.3 86.4 %all-gather.9.cloned.1.call-start = ((), (), s32[]{:S(2)}) async-start(), calls=%async_computation.2 | async-start | bytes 1179648 | tf_op jit(solution)/shard_map/all_gather | solution.py:31
  8.0 126.8 %all-gather.7.cloned.1.call-start = ((), (), s32[]{:S(2)}) async-start(), calls=%async_computation.1 | async-start | bytes 1179648 | tf_op jit(solution)/shard_map/all_gather | solution.py:30
  8.7 178.1 %all-gather.13.cloned.1.call-start = ((), (), s32[]{:S(2)}) async-start(), calls=%async_computation.4 | async-start | bytes 2359296 | tf_op jit(solution)/shard_map/all_gather | solution.py:14
  38.9 101.3 %copy-start.1 = (f32[4]{0:T(128)S(1)}, f32[4]{0:T(128)}, u32[]{:S(2)}) copy-start(f32[4]{0:T(128)} %param.15) | copy-start | bytes 52
  138.7 97.9 %all-gather.15.cloned.1.call-start = ((), (), s32[]{:S(2)}) async-start(), calls=%async_computation.5 | async-start | bytes 2359296 | tf_op jit(solution)/shard_map/all_gather | solution.py:14
  139.6 136.9 %all-gather.17.cloned.1.call-start = ((), (), s32[]{:S(2)}) async-start(), calls=%async_computation.6 | async-start | bytes 1179648 | tf_op jit(solution)/shard_map/all_gather | solution.py:94
  140.2 162.9 %reduce-scatter.2.cloned.1.call-start = ((), (), s32[]{:S(2)}) async-start(), calls=%async_computation.7 | async-start | bytes 1310720 | tf_op jit(solution)/shard_map/reduce_scatter | solution.py:20
  236.6 67.6 %copy-start = (f32[1024]{0:T(1024)S(1)}, f32[1024]{0:T(1024)}, u32[]{:S(2)}) copy-start(f32[1024]{0:T(1024)} %param.17) | copy-start | bytes 12292
  237.0 7.9 %copy-start.2 = (bf16[2048,4,128]{2,0,1:T(8,128)(2,1)S(1)}, bf16[2048,4,128]{2,0,1:T(8,128)(2,1)}, u32[]{:S(2)}) copy-start(bf16[2048,4,128]{2,0,1:T(8,128)(2,1)} %get-tuple-element.28) | copy-start | bytes 6291460 | tf_op jit(solution)/shard_map/cond
Sparse Core Ops, SparseCore 0:
  9.5 42.9 all-gather.10
  54.6 38.9 all-gather.8
  95.8 38.9 all-gather.6
  138.8 48.0 all-gather.12
  188.9 47.6 all-gather.14
  238.5 37.9 all-gather.16
  279.3 23.7 reduce-scatter.1
where the time goes:
time: 313 us
  waiting for transfers between devices  214 us (68%)
  blocking collectives  61 us (19%)
  between operations  13.6 us (4%)
  matrix products  13.5 us (4%)
  other arithmetic  7.89 us (3%)
    all_gather x2, waiting for transfers between devices, over_all(): lax.all_gather(a, axis, axis=dim, tiled=True)  63.7 us
    all_gather x1, waiting for transfers between devices, on_device(): whole_q = lax.all_gather(query_weight, 'sp', axis=0, tiled=True)  41.2 us
    all_gather x1, waiting for transfers between devices, on_device(): whole_k = lax.all_gather(key_weight, 'sp', axis=0, tiled=True)  41.1 us
    all_gather x1, blocking collectives, on_device(): gates_all = lax.all_gather(log_gate, 'sp', axis=0, tiled=True)  31 us
    all_gather x1, waiting for transfers between devices, on_device(): out_full = lax.all_gather(out_weight, 'sp', axis=1, tiled=True)  28 us
    reduce_scatter x1, waiting for transfers between devices, own_rows(): own = lax.psum_scatter(everything, axis, scatter_dimension=0, tiled=True)  24 us
    all_gather x1, blocking collectives, on_device(): whole_g = lax.all_gather(gate_weight, 'sp', axis=0, tiled=True)  22.6 us
    all_gather x1, waiting for transfers between devices, on_device(): whole_v = lax.all_gather(value_weight, 'sp', axis=0, tiled=True)  13.5 us
  transfers between devices with their start and end apart: 7, of which 7 were waited for; matrix products, arithmetic and copies ran while one was open for 5% of the time, Pallas kernels for 0%

commit v1 on v0

--- a/solution.py
+++ b/solution.py
@@ -27,8 +27,13 @@
     width = query_weight.shape[1]
     heads = gate_weight.shape[1]
     head_size = width // heads
-    whole_q = lax.all_gather(query_weight, "sp", axis=0, tiled=True)
-    whole_k = lax.all_gather(key_weight, "sp", axis=0, tiled=True)
+    whole_q, whole_k = jnp.split(
+        lax.all_gather(
+            jnp.concatenate([query_weight, key_weight], axis=1), "sp", axis=0, tiled=True
+        ),
+        [query_weight.shape[1]],
+        axis=1,
+    )
     whole_v = lax.all_gather(value_weight, "sp", axis=0, tiled=True)
     whole_g = lax.all_gather(gate_weight, "sp", axis=0, tiled=True)
     joined = jnp.concatenate([whole_q, whole_k, whole_v, whole_g], axis=1)

time: 313 us -> 280 us (0.89)
  waiting for transfers between devices: 214 us -> 180 us
    all_gather x2 -> x1, waiting for transfers between devices: 82.3 us -> 50 us  [on_device(): lax.all_gather(jnp.concatenate([query_weight, key_weight], axis=1), 'sp',...]
  transfers between devices with their start and end apart: 7 -> 6, of which waited for: 7 -> 6; matrix products, arithmetic and copies ran while one was open for 5% -> 6% of each run, Pallas kernels for 0% -> 0%
where the time goes in v1:
time: 280 us
  waiting for transfers between devices  180 us (64%)
  blocking collectives  61 us (22%)
  matrix products  13.6 us (5%)
  between operations  13.6 us (5%)
  other arithmetic  9.58 us (3%)
    all_gather x2, waiting for transfers between devices, over_all(): lax.all_gather(a, axis, axis=dim, tiled=True)  63.3 us
    all_gather x1, waiting for transfers between devices, on_device(): lax.all_gather(jnp.concatenate([query_weight, key_weight], axis=1), 'sp',...  50 us
    all_gather x1, blocking collectives, on_device(): gates_all = lax.all_gather(log_gate, 'sp', axis=0, tiled=True)  31 us
    all_gather x1, waiting for transfers between devices, on_device(): out_full = lax.all_gather(out_weight, 'sp', axis=1, tiled=True)  28 us
    reduce_scatter x1, waiting for transfers between devices, own_rows(): own = lax.psum_scatter(everything, axis, scatter_dimension=0, tiled=True)  24 us
    all_gather x1, blocking collectives, on_device(): whole_g = lax.all_gather(gate_weight, 'sp', axis=0, tiled=True)  22.6 us
    all_gather x1, waiting for transfers between devices, on_device(): whole_v = lax.all_gather(value_weight, 'sp', axis=0, tiled=True)  13.3 us
    all_gather x1, blocking collectives, on_whole(): whole = lax.all_gather(shard, axis, axis=dim, tiled=True)  7.38 us
  transfers between devices with their start and end apart: 6, of which 6 were waited for; matrix products, arithmetic and copies ran while one was open for 6% of the time, Pallas kernels for 0%

profile of v1, /device:TPU:0, one launch (start us, length us, event | category | flops | bytes accessed | tf_op | source)
XLA Modules:
  0.0 280.1 jit_solution(13188903965643147000)
XLA Ops:
  6.5 0.0 all-gather.8.cloned.1.call-start
  6.5 0.7 all-gather.8.cloned.1.call-update
  7.3 0.0 all-gather.6.cloned.1.call-start
  7.3 1.7 pad_maximum_fusion
  9.0 0.0 all-gather.6.cloned.1.call-update
  9.0 0.0 all-gather.10.cloned.1.call-start
  9.1 22.6 %all_gather.26 = bf16[1024,4]{0,1:T(4,128)(2,1)S(1)} all-gather(bf16[128,4]{0,1:T(4,128)(2,1)} %param.14), channel_id=1, replica_groups=mesh['sp'=8,'tp'=4] {'sp'}, dimensions={0}, use_global_device_ids=true | all-gather | bytes 9216 | tf_op jit(solution)/shard_map/all_gather | solution.py:38
  31.6 0.2 copy.14
  31.8 7.4 %all_gather.27 = bf16[256,1024]{1,0:T(8,128)(2,1)S(1)} all-gather(bf16[64,1024]{1,0:T(8,128)(2,1)} %param.10), channel_id=1, replica_groups=mesh['sp'=8,'tp'=4] {'tp'}, dimensions={0}, use_global_device_ids=true | all-gather | bytes 655360 | tf_op jit(solution)/shard_map/all_gather | solution.py:9
  39.2 0.0 copy-start.1
  39.2 13.3 %all-gather.8.cloned.1.call-done = bf16[1024,512]{1,0:T(8,128)(2,1)} async-done(((bf16[128,512]{1,0:T(8,128)(2,1)}), bf16[1024,512]{1,0:T(8,128)(2,1)}) %all-gather.8.cloned.1.call-update) | async-done | bytes 1048592 | tf_op jit(solution)/shard_map/all_gather | solution.py:37
  52.5 50.0 %all-gather.6.cloned.1.call-done = bf16[1024,1024]{1,0:T(8,128)(2,1)} async-done(((bf16[128,1024]{1,0:T(8,128)(2,1)}), bf16[1024,1024]{1,0:T(8,128)(2,1)}) %all-gather.6.cloned.1.call-update) | async-done | bytes 2097168 | tf_op jit(solution)/shard_map/all_gather | solution.py:31
  102.5 3.0 %fusion.30 = (bf16[256,1540]{0,1:T(8,128)(2,1)S(1)}, f32[256,1540]{0,1:T(8,128)S(1)}) fusion(bf16[256,1024]{1,0:T(8,128)(2,1)S(1)} %all_gather.27, bf16[1024,4]{1,0:T(8,128)(2,1)S(1)} %copy.14, bf16[1024,512]{1,0:T(8,128)(2,1)} %all-gather.8.cloned.1.call-done, bf16[1024,1024]{1,0:T(8,128)(2,1)} %all-gather.6.cloned.1.call-done), kind=kOutput, calls=%fused_computation.46 | convolution fusion | flops 817259520 | bytes 6043648 | tf_op jit(solution)/shard_map/dot_general | solution.py:42
  105.5 0.8 copy.15
  106.4 0.0 all-gather.10.cloned.1.call-update
  106.4 0.0 all-gather.12.cloned.1.call-start
  106.4 0.9 copy.16
  107.3 0.0 all-gather.12.cloned.1.call-update
  107.3 0.0 all-gather.14.cloned.1.call-start
  107.4 0.5 all-gather.14.cloned.1.call-update
  107.9 0.0 reduce-scatter.2.cloned.1.call-start
  108.0 0.0 copy-done.1
  108.0 0.1 fusion.24
  108.1 31.0 %all_gather.29 = f32[2048,4]{0,1:T(4,128)S(1)} all-gather(f32[256,4]{0,1:T(4,128)S(1)} %fusion.24), channel_id=1, replica_groups=mesh['sp'=8,'tp'=4] {'sp'}, dimensions={0}, use_global_device_ids=true | all-gather | bytes 36864 | tf_op jit(solution)/shard_map/all_gather | solution.py:53
  139.1 1.1 reduce-window.6
  140.2 0.2 slice_reduce_fusion
  140.4 0.2 reduce-window.9
  140.6 0.1 add_bitcast_fusion
  140.7 13.6 %all-gather.10.cloned.1.call-done = bf16[2048,4,128]{2,0,1:T(8,128)(2,1)} async-done(((bf16[256,4,128]{2,0,1:T(8,128)(2,1)}), bf16[2048,4,128]{2,0,1:T(8,128)(2,1)}) %all-gather.10.cloned.1.call-update) | async-done | bytes 2097168 | tf_op jit(solution)/shard_map/all_gather | solution.py:14
  154.3 49.7 %all-gather.12.cloned.1.call-done = bf16[2048,4,128]{2,0,1:T(8,128)(2,1)} async-done(((bf16[256,4,128]{2,0,1:T(8,128)(2,1)}), bf16[2048,4,128]{2,0,1:T(8,128)(2,1)}) %all-gather.12.cloned.1.call-update) | async-done | bytes 2097168 | tf_op jit(solution)/shard_map/all_gather | solution.py:14
  204.0 0.0 copy-start
  204.0 11.8 %conditional.1 = (f32[4,256]{1,0:T(4,128)S(1)}, f32[4,256,128]{1,2,0:T(8,128)S(1)}) conditional(s32[]{:T(128)} %convert_element_type.19, (s32[]{:T(128)}, s32[256]{0:T(256)S(1)}, bf16[256,1540]{0,1:T(8,128)(2,1)S(1)}, bf16[2048,4,128]{2,0,1:T(8,128)(2,1)}, f32[256,4]{0,1:T(4,128)S(1)}, /*index=5*/f32[2048,4]{0,1:T(4,128)S(1)}, ...), branch_computations={%region_2.5_spmd, %region_5.6_spmd} | conditional | flops 1112149248 | bytes 42363952 | solution.py:83
  204.0 0.4 iota_compare_fusion
  204.4 0.0 copy-start.2
  204.4 4.6 %fusion.2 = (f32[4,256]{1,0:T(4,128)S(1)}, f32[4,256,2048]{2,1,0:T(8,128)S(1)}) fusion(f32[4,2048]{1,0:T(4,128)S(1)} %bitcast.40, f32[4,256]{1,0:T(4,128)S(1)} %bitcast.45, pred[256,2048]{1,0:T(8,128)(4,1)S(1)} %iota_compare_fusion, bf16[256,4,128]{0,2,1:T(8,128)(2,1)S(1)} %bitcast.37, bf16[2048,4,128]{2,0,1:T(8,128)(2,1)} %get-tuple-element.25), kind=kOutput, calls=%fused_computation.4 | convolution fusion | flops 547355648 | bytes 11313152 | tf_op jit(solution)/shard_map/cond/branch_0_fun/qhd,khd->hqk/dot_general | solution.py:66
  209.0 3.2 %fusion.1 = f32[4,256]{1,0:T(4,128)S(1)} fusion(f32[4,256,2048]{2,1,0:T(8,128)S(1)} %get-tuple-element.45, f32[4,256]{1,0:T(4,128)S(1)} %broadcast_maximum_fusion, f32[4,2048]{1,0:T(4,128)S(1)} %bitcast.41, f32[4,256]{1,0:T(4,128)S(1)} %bitcast.46, pred[256,2048]{1,0:T(8,128)(4,1)S(1)} %iota_compare_fusion), kind=kLoop, calls=%fused_computation.3 | loop fusion | flops 14679040 | bytes 8957952 | tf_op jit(solution)/shard_map/cond/branch_0_fun/reduce_sum | solution.py:76
  212.3 0.0 copy-done.2
  212.3 3.3 %fusion.10 = f32[4,256,128]{2,1,0:T(8,128)S(1)} fusion(bf16[2048,4,128]{2,0,1:T(8,128)(2,1)S(1)} %copy-done.2, f32[4,256,2048]{2,1,0:T(8,128)S(1)} %get-tuple-element.45, f32[4,256]{1,0:T(4,128)S(1)} %broadcast_maximum_fusion, f32[4,2048]{1,0:T(4,128)S(1)} %bitcast.42, f32[4,256]{1,0:T(4,128)S(1)} %bitcast.47, pred[256,2048]{1,0:T(8,128)(4,1)S(1)} %iota_compare_fusion, ...), kind=kOutput, calls=%fused_computation.13 | convolution fusion | flops 549584896 | bytes 11579392 | tf_op jit(solution)/shard_map/cond/branch_0_fun/hqk,khd->hqd/dot_general | solution.py:77
  215.5 0.2 copy.19
  215.8 28.0 %all-gather.14.cloned.1.call-done = bf16[512,1024]{1,0:T(8,128)(2,1)} async-done(((bf16[512,128]{1,0:T(8,128)(2,1)}), bf16[512,1024]{1,0:T(8,128)(2,1)}) %all-gather.14.cloned.1.call-update) | async-done | bytes 1048592 | tf_op jit(solution)/shard_map/all_gather | solution.py:99
  243.8 2.7 fusion.31
  246.5 0.0 reduce-scatter.2.cloned.1.call-update
  246.5 24.0 %reduce-scatter.2.cloned.1.call-done = f32[64,1024]{1,0:T(8,128)} async-done(((f32[256,1024]{1,0:T(8,128)}), f32[64,1024]{1,0:T(8,128)}) %reduce-scatter.2.cloned.1.call-update) | async-done | bytes 262160 | tf_op jit(solution)/shard_map/reduce_scatter | solution.py:20
  270.5 1.1 multiply_reduce_fusion
  271.6 0.0 copy-done
  271.6 1.7 multiply_convert_fusion
  (11 shorter events, 0.2 us)
Async XLA Ops:
  6.5 46.0 %all-gather.8.cloned.1.call-start = ((), (), s32[]{:S(2)}) async-start(), calls=%async_computation.2 | async-start | bytes 1179648 | tf_op jit(solution)/shard_map/all_gather | solution.py:37
  7.3 95.2 %all-gather.6.cloned.1.call-start = ((), (), s32[]{:S(2)}) async-start(), calls=%async_computation.1 | async-start | bytes 2359296 | tf_op jit(solution)/shard_map/all_gather | solution.py:31
  9.0 145.3 %all-gather.10.cloned.1.call-start = ((), (), s32[]{:S(2)}) async-start(), calls=%async_computation.3 | async-start | bytes 2359296 | tf_op jit(solution)/shard_map/all_gather | solution.py:14
  39.2 68.7 %copy-start.1 = (f32[4]{0:T(128)S(1)}, f32[4]{0:T(128)}, u32[]{:S(2)}) copy-start(f32[4]{0:T(128)} %param.15) | copy-start | bytes 52
  106.4 97.6 %all-gather.12.cloned.1.call-start = ((), (), s32[]{:S(2)}) async-start(), calls=%async_computation.4 | async-start | bytes 2359296 | tf_op jit(solution)/shard_map/all_gather | solution.py:14
  107.3 136.5 %all-gather.14.cloned.1.call-start = ((), (), s32[]{:S(2)}) async-start(), calls=%async_computation.5 | async-start | bytes 1179648 | tf_op jit(solution)/shard_map/all_gather | solution.py:99
  107.9 162.6 %reduce-scatter.2.cloned.1.call-start = ((), (), s32[]{:S(2)}) async-start(), calls=%async_computation.6 | async-start | bytes 1310720 | tf_op jit(solution)/shard_map/reduce_scatter | solution.py:20
  204.0 67.6 %copy-start = (f32[1024]{0:T(1024)S(1)}, f32[1024]{0:T(1024)}, u32[]{:S(2)}) copy-start(f32[1024]{0:T(1024)} %param.17) | copy-start | bytes 12292
  204.4 7.9 %copy-start.2 = (bf16[2048,4,128]{2,0,1:T(8,128)(2,1)S(1)}, bf16[2048,4,128]{2,0,1:T(8,128)(2,1)}, u32[]{:S(2)}) copy-start(bf16[2048,4,128]{2,0,1:T(8,128)(2,1)} %get-tuple-element.28) | copy-start | bytes 6291460 | tf_op jit(solution)/shard_map/cond
Sparse Core Ops, SparseCore 0:
  9.5 43.0 all-gather.7
  54.6 47.7 all-gather.5
  106.5 47.7 all-gather.9
  156.3 47.6 all-gather.11
  205.9 37.9 all-gather.13
  246.7 23.7 reduce-scatter.1
